TPU v7x, 32 devices: a whole 2x2x4 slice. The times are simulated.
32 devices in a mesh: rep: 2 (over x), fs: 8 (over z, y), tp: 2 (over core).
Axes of the slice: x: 2, y: 2, z: 4, core: 2. Of those that a mesh axis runs over, the one named last changes fastest.
Arguments:
- stream: bfloat16 [6144, 2048], P(('rep', 'fs'), 'tp'), may hold values from -24 to 24
- recurrence_input_weight: bfloat16 [2048, 2048], P('fs', 'tp'), may hold values from -0.125 to 0.125
- output_gate_weight: bfloat16 [2048, 2048], P('fs', 'tp'), may hold values from -0.125 to 0.125
- recurrence_gate_matrix: bfloat16 [16, 128, 128], P('tp'), may hold values from -0.5 to 0.5
- input_gate_matrix: bfloat16 [16, 128, 128], P('tp'), may hold values from -0.5 to 0.5
- channel_decay_rate: float32 [2048], P('tp')
- recurrence_taps: float32 [4, 2048], P(None, 'tp'), may hold values from -3 to 3
- spike_log_decay: float32 [6144, 16], P(('rep', 'fs'), 'tp'), may hold values from -2.1 to 0
- recurrence_output_weight: bfloat16 [2048, 2048], P('tp', 'fs'), may hold values from -0.3125 to 0.3125
- feedforward_gate_upward: bfloat16 [2048, 4096], P('fs', 'tp'), may hold values from -0.125 to 0.125
- feedforward_value_upward: bfloat16 [2048, 4096], P('fs', 'tp'), may hold values from -0.125 to 0.125
- feedforward_gate_taps: float32 [3, 4096], P(None, 'tp'), may hold values from -3 to 3
- feedforward_value_taps: float32 [3, 4096], P(None, 'tp'), may hold values from -3 to 3
- feedforward_down_weight: bfloat16 [4096, 2048], P('tp', 'fs'), may hold values from -0.1875 to 0.1875
- recurrence_norm_gain: float32 [2048], replicated, may hold values from 0.1 to 1.9
- feedforward_norm_gain: float32 [2048], replicated, may hold values from 0.1 to 1.9
- closing_norm_gain: float32 [2048], replicated, may hold values from 0.1 to 1.9
Outputs:
- layer_out: bfloat16 [6144, 2048], P(('rep', 'fs'), 'tp')
All inputs are finite; a program needn't handle non-finite values.
Results may differ from a plain program's by a relative error of at most 0.018.
Values may be sent and summed in bfloat16 or wider, within the bound.
A program may use at most 64 MiB of HBM per device.

v0:
```python
import jax
import jax.numpy as jnp
from jax import lax
from jax.sharding import PartitionSpec as P

EPS = 1e-06
GATE_POWER = 8.0


def rms_scale(row_block, gain_vec):
    widened = row_block.astype(jnp.float32)
    inverse = lax.rsqrt(jnp.mean(widened * widened, axis=-1, keepdims=True) + EPS)
    return (widened * inverse * gain_vec).astype(jnp.bfloat16)


def causal_mix(values, kernel_taps):
    extent = kernel_taps.shape[0]
    length = values.shape[0]
    padded = jnp.pad(values, ((extent - 1, 0), (0, 0)))
    summed = kernel_taps[0] * padded[0:length]
    for offset in range(1, extent):
        summed = summed + kernel_taps[offset] * padded[offset : offset + length]
    return summed


def chain_step(earlier, following):
    return (earlier[0] * following[0], following[0] * earlier[1] + following[1])


def fold_pair(source, pieces):
    return (
        jnp.dot(source, pieces[0], preferred_element_type=jnp.float32),
        jnp.dot(source, pieces[1], preferred_element_type=jnp.float32),
    )


def project_with(left_rows, weight_piece):
    return jnp.dot(left_rows, weight_piece, preferred_element_type=jnp.float32).astype(jnp.bfloat16)


def shards(
    stream,
    recurrence_input_weight,
    output_gate_weight,
    recurrence_gate_matrix,
    input_gate_matrix,
    channel_decay_rate,
    recurrence_taps,
    spike_log_decay,
    recurrence_output_weight,
    feedforward_gate_upward,
    feedforward_value_upward,
    feedforward_gate_taps,
    feedforward_value_taps,
    feedforward_down_weight,
    recurrence_norm_gain,
    feedforward_norm_gain,
    closing_norm_gain,
):
    tok_rows = stream.shape[0]
    head_count = recurrence_gate_matrix.shape[0]
    block_size = recurrence_gate_matrix.shape[1]
    whole_rows = lax.all_gather(stream, "tp", axis=1, tiled=True)
    normed = rms_scale(whole_rows, recurrence_norm_gain)
    rec_sum, gate_sum = fold_pair(
        normed,
        (
            lax.all_gather(recurrence_input_weight, "fs", axis=0, tiled=True),
            lax.all_gather(output_gate_weight, "fs", axis=0, tiled=True),
        ),
    )
    rec_in = rec_sum.astype(jnp.bfloat16)
    gate_src = gate_sum.astype(jnp.bfloat16)
    conv_out = causal_mix(rec_in.astype(jnp.float32), recurrence_taps).astype(jnp.bfloat16)
    blocks = conv_out.reshape(tok_rows, head_count, block_size)
    gate_restart = jax.nn.sigmoid(
        jnp.einsum(
            "thi,hij->thj", blocks, recurrence_gate_matrix, preferred_element_type=jnp.float32
        )
    )
    admit_gate = jax.nn.sigmoid(
        jnp.einsum("thi,hij->thj", blocks, input_gate_matrix, preferred_element_type=jnp.float32)
    )
    decay_base = (GATE_POWER * jax.nn.softplus(-channel_decay_rate)).reshape(head_count, block_size)
    decay_logarithm = -gate_restart * decay_base + spike_log_decay[:, :, None]
    decay_rate = jnp.exp(decay_logarithm)
    inflow = jnp.sqrt(-jnp.expm1(2.0 * decay_logarithm)) * admit_gate * blocks.astype(jnp.float32)
    states = lax.associative_scan(chain_step, (decay_rate, inflow), axis=0)[1]
    mixed_out = (
        states.reshape(tok_rows, head_count * block_size)
        * jax.nn.gelu(gate_src.astype(jnp.float32))
    ).astype(jnp.bfloat16)
    mix_terms = project_with(
        mixed_out, lax.all_gather(recurrence_output_weight, "fs", axis=1, tiled=True)
    )
    branch = lax.psum_scatter(
        lax.optimization_barrier(mix_terms).astype(jnp.float32).astype(jnp.bfloat16),
        "tp",
        scatter_dimension=1,
        tiled=True,
    )
    middle = (stream.astype(jnp.float32) + branch.astype(jnp.float32)).astype(jnp.bfloat16)
    whole_middle = lax.all_gather(middle, "tp", axis=1, tiled=True)
    normed_ffn = rms_scale(whole_middle, feedforward_norm_gain)
    gate_sum_ffn, value_sum_ffn = fold_pair(
        normed_ffn,
        (
            lax.all_gather(feedforward_gate_upward, "fs", axis=0, tiled=True),
            lax.all_gather(feedforward_value_upward, "fs", axis=0, tiled=True),
        ),
    )
    gate_up = gate_sum_ffn.astype(jnp.bfloat16)
    value_up = value_sum_ffn.astype(jnp.bfloat16)
    gate_conv = causal_mix(gate_up.astype(jnp.float32), feedforward_gate_taps)
    value_conv = causal_mix(value_up.astype(jnp.float32), feedforward_value_taps)
    hidden = (jax.nn.gelu(gate_conv) * value_conv).astype(jnp.bfloat16)
    down_terms = project_with(
        hidden, lax.all_gather(feedforward_down_weight, "fs", axis=1, tiled=True)
    )
    branch_ffn = lax.psum_scatter(
        lax.optimization_barrier(down_terms).astype(jnp.float32).astype(jnp.bfloat16),
        "tp",
        scatter_dimension=1,
        tiled=True,
    )
    final_rows = middle.astype(jnp.float32) + branch_ffn.astype(jnp.float32)
    col_count = final_rows.shape[1]
    square_sum = lax.psum(jnp.sum(final_rows * final_rows, axis=1), "tp")
    inverse = lax.rsqrt(square_sum / (col_count * lax.axis_size("tp")) + EPS)
    gain_part = lax.dynamic_slice_in_dim(
        closing_norm_gain, lax.axis_index("tp") * col_count, col_count
    )
    return (final_rows * inverse[:, None] * gain_part[None, :]).astype(jnp.bfloat16)


def solution(mesh):
    in_specs = (
        P(("rep", "fs"), "tp"),
        P("fs", "tp"),
        P("fs", "tp"),
        P("tp", None, None),
        P("tp", None, None),
        P("tp"),
        P(None, "tp"),
        P(("rep", "fs"), "tp"),
        P("tp", "fs"),
        P("fs", "tp"),
        P("fs", "tp"),
        P(None, "tp"),
        P(None, "tp"),
        P("tp", "fs"),
        P(),
        P(),
        P(),
    )
    out_specs = P(("rep", "fs"), "tp")
    return jax.shard_map(shards, mesh=mesh, in_specs=in_specs, out_specs=out_specs, check_vma=False)
```

profile of v0, /device:TPU:0, one launch (start us, length us, event | category | flops | bytes accessed | tf_op | source)
XLA Modules:
  0.0 688.8 jit_solution(16503987164098844591)
XLA Ops:
  9.4 12.0 %all-gather.9.cloned.1.call-done = bf16[384,2048]{1,0:T(8,128)(2,1)} async-done(((bf16[384,1024]{1,0:T(8,128)(2,1)}), bf16[384,2048]{1,0:T(8,128)(2,1)}) %all-gather.9.cloned.1.call-update) | async-done | bytes 1572880 | tf_op jit(solution)/shard_map/all_gather | solution.py:63
  21.4 1.9 fusion
  23.4 74.2 %all-gather.11.cloned.1.call-done = bf16[2048,1024]{1,0:T(8,128)(2,1)} async-done(((bf16[256,1024]{1,0:T(8,128)(2,1)}), bf16[2048,1024]{1,0:T(8,128)(2,1)}) %all-gather.11.cloned.1.call-update) | async-done | bytes 4194320 | tf_op jit(solution)/shard_map/all_gather | solution.py:68
  97.6 4.0 fusion.36
  111.0 2.0 fusion.67
  118.9 2.3 fusion.68
  121.2 1.7 slice.265
  122.9 1.7 slice.266
  124.6 1.7 slice.264
  126.2 1.7 slice.268
  127.9 1.9 fusion.69
  131.1 1.7 slice.270
  134.3 1.7 fusion.70
  160.4 1.7 slice.263
  162.0 1.7 slice.306
  177.5 3.9 pad.76
  183.9 3.8 pad.75
  189.1 1.9 copy.24
  192.7 53.4 %all-gather.15.cloned.1.call-done = bf16[1024,2048]{1,0:T(8,128)(2,1)} async-done(((bf16[1024,256]{1,0:T(8,128)(2,1)}), bf16[1024,2048]{1,0:T(8,128)(2,1)}) %all-gather.15.cloned.1.call-update) | async-done | bytes 4194320 | tf_op jit(solution)/shard_map/all_gather | solution.py:94
  246.2 8.8 %convolution_convert_fusion.3 = bf16[384,2048]{1,0:T(8,128)(2,1)} fusion(bf16[1024,2048]{1,0:T(8,128)(2,1)} %all-gather.15.cloned.1.call-done, f32[384,1024]{1,0:T(8,128)} %copy.25, bf16[2048,1024]{1,0:T(8,128)(2,1)} %all-gather.13.cloned.1.call-done, bf16[384,2048]{1,0:T(8,128)(2,1)S(1)} %copy-done.8, f32[2048]{0:T(1024)S(1)} %copy-done.37, ...), kind=kOutput, calls=%fused_computation.23 | convolution fusion | flops 3229876224 | bytes 13116928 | tf_op jit(solution)/shard_map/dot_general | solution.py:38
  255.3 7.1 %reduce-scatter.3.cloned.1.call-done = bf16[384,1024]{1,0:T(8,128)(2,1)} async-done(((bf16[384,2048]{1,0:T(8,128)(2,1)}), bf16[384,1024]{1,0:T(8,128)(2,1)}) %reduce-scatter.3.cloned.1.call-update) | async-done | bytes 786448 | tf_op jit(solution)/shard_map/reduce_scatter | solution.py:96
  262.3 2.3 add_convert_fusion
  267.1 8.8 %all-gather.17.cloned.1.call-done = bf16[384,2048]{1,0:T(8,128)(2,1)} async-done(((bf16[384,1024]{1,0:T(8,128)(2,1)}), bf16[384,2048]{1,0:T(8,128)(2,1)}) %all-gather.17.cloned.1.call-update) | async-done | bytes 1572880 | tf_op jit(solution)/shard_map/all_gather | solution.py:103
  275.9 1.9 fusion.3
  277.8 125.9 %all-gather.19.cloned.1.call-done = bf16[2048,2048]{1,0:T(8,128)(2,1)} async-done(((bf16[256,2048]{1,0:T(8,128)(2,1)}), bf16[2048,2048]{1,0:T(8,128)(2,1)}) %all-gather.19.cloned.1.call-update) | async-done | bytes 8388624 | tf_op jit(solution)/shard_map/all_gather | solution.py:108
  403.7 8.5 %fusion.15 = f32[384,2048]{1,0:T(8,128)} fusion(bf16[2048,2048]{1,0:T(8,128)(2,1)} %all-gather.19.cloned.1.call-done, bf16[384,2048]{1,0:T(8,128)(2,1)S(1)} %copy-done.9, f32[2048]{0:T(1024)S(1)} %copy-done.38, f32[384]{0:T(512)S(1)} %add_rsqrt_fusion.1), kind=kOutput, calls=%fused_computation.24 | convolution fusion | flops 3225944064 | bytes 13116928 | tf_op jit(solution)/shard_map/dot_general | solution.py:32
  412.2 116.3 %all-gather.21.cloned.1.call-done = bf16[2048,2048]{1,0:T(8,128)(2,1)} async-done(((bf16[256,2048]{1,0:T(8,128)(2,1)}), bf16[2048,2048]{1,0:T(8,128)(2,1)}) %all-gather.21.cloned.1.call-update) | async-done | bytes 8388624 | tf_op jit(solution)/shard_map/all_gather | solution.py:109
  528.5 8.5 %fusion.16 = f32[384,2048]{1,0:T(8,128)} fusion(bf16[2048,2048]{1,0:T(8,128)(2,1)} %all-gather.21.cloned.1.call-done, bf16[384,2048]{1,0:T(8,128)(2,1)S(1)} %copy-done.9, f32[2048]{0:T(1024)S(1)} %copy-done.38, f32[384]{0:T(512)S(1)} %add_rsqrt_fusion.1), kind=kOutput, calls=%fused_computation.25 | convolution fusion | flops 3225944064 | bytes 13116928 | tf_op jit(solution)/shard_map/dot_general | solution.py:33
  537.0 116.7 %all-gather.23.cloned.1.call-done = bf16[2048,2048]{1,0:T(8,128)(2,1)} async-done(((bf16[2048,256]{1,0:T(8,128)(2,1)}), bf16[2048,2048]{1,0:T(8,128)(2,1)}) %all-gather.23.cloned.1.call-update) | async-done | bytes 8388624 | tf_op jit(solution)/shard_map/all_gather | solution.py:118
  653.7 15.7 %convolution_convert_fusion = bf16[384,2048]{1,0:T(8,128)(2,1)} fusion(bf16[2048,2048]{1,0:T(8,128)(2,1)} %all-gather.23.cloned.1.call-done, f32[384,2048]{1,0:T(8,128)} %fusion.16, f32[384,2048]{1,0:T(8,128)} %fusion.15, f32[2048]{0:T(1024)S(1)} %bitcast.45, f32[2048]{0:T(1024)S(1)} %bitcast.46, f32[2048]{0:T(1024)S(1)} %bitcast.44, ...), kind=kOutput, calls=%fused_computation.20 | convolution fusion | flops 3237740544 | bytes 16302080 | tf_op jit(solution)/shard_map/dot_general | solution.py:38
  669.5 7.3 %reduce-scatter.5.cloned.1.call-done = bf16[384,1024]{1,0:T(8,128)(2,1)} async-done(((bf16[384,2048]{1,0:T(8,128)(2,1)}), bf16[384,1024]{1,0:T(8,128)(2,1)}) %reduce-scatter.5.cloned.1.call-update) | async-done | bytes 786448 | tf_op jit(solution)/shard_map/reduce_scatter | solution.py:120
  678.3 2.5 psum.7
  (196 shorter events, 69.5 us)
Async XLA Ops:
  6.5 95.8 %copy-start = (bf16[8,128,128]{2,1,0:T(8,128)(2,1)S(1)}, bf16[8,128,128]{2,1,0:T(8,128)(2,1)}, u32[]{:S(2)}) copy-start(bf16[8,128,128]{2,1,0:T(8,128)(2,1)} %param.20) | copy-start | bytes 786436
  6.5 14.9 %all-gather.9.cloned.1.call-start = ((), (), s32[]{:S(2)}) async-start(), calls=%async_computation.2 | async-start | bytes 2359296 | tf_op jit(solution)/shard_map/all_gather | solution.py:63
  7.3 90.3 %copy-start.36 = (f32[2048]{0:T(1024)S(1)}, f32[2048]{0:T(1024)}, u32[]{:S(2)}) copy-start(f32[2048]{0:T(1024)} %param.31) | copy-start | bytes 24580
  7.3 90.3 %all-gather.11.cloned.1.call-start = ((), (), s32[]{:S(2)}) async-start(), calls=%async_computation.3 | async-start | bytes 4718592 | tf_op jit(solution)/shard_map/all_gather | solution.py:68
  8.0 184.7 %all-gather.13.cloned.1.call-start = ((), (), s32[]{:S(2)}) async-start(), calls=%async_computation.4 | async-start | bytes 4718592 | tf_op jit(solution)/shard_map/all_gather | solution.py:69
  8.8 237.4 %all-gather.15.cloned.1.call-start = ((), (), s32[]{:S(2)}) async-start(), calls=%async_computation.5 | async-start | bytes 4718592 | tf_op jit(solution)/shard_map/all_gather | solution.py:94
  9.3 253.0 %reduce-scatter.3.cloned.1.call-start = ((), (), s32[]{:S(2)}) async-start(), calls=%async_computation.6 | async-start | bytes 2359296 | tf_op jit(solution)/shard_map/reduce_scatter | solution.py:96
  21.4 76.1 %copy-start.7 = (bf16[384,2048]{1,0:T(8,128)(2,1)S(1)}, bf16[384,2048]{1,0:T(8,128)(2,1)}, u32[]{:S(2)}) copy-start(bf16[384,2048]{1,0:T(8,128)(2,1)} %all-gather.9.cloned.1.call-done) | copy-start | bytes 4718596
  23.4 78.2 %copy-start.32 = (f32[384]{0:T(512)}, f32[384]{0:T(512)S(1)}, u32[]{:S(2)}) copy-start(f32[384]{0:T(512)S(1)} %add_rsqrt_fusion.2) | copy-start | bytes 4612
  103.4 6.1 copy-start.3
  168.6 3.8 copy-start.17
  168.6 3.8 copy-start.18
  168.6 4.0 copy-start.19
  168.6 4.0 copy-start.20
  168.6 4.1 copy-start.29
  168.6 4.2 copy-start.15
  168.6 4.2 copy-start.28
  191.0 55.1 %copy-start.8 = (bf16[384,2048]{1,0:T(8,128)(2,1)S(1)}, bf16[384,2048]{1,0:T(8,128)(2,1)}, u32[]{:S(2)}) copy-start(bf16[384,2048]{1,0:T(8,128)(2,1)} %all-gather.9.cloned.1.call-done) | copy-start | bytes 4718596
  191.0 55.1 %copy-start.33 = (f32[384]{0:T(512)S(1)}, f32[384]{0:T(512)}, u32[]{:S(2)}) copy-start(f32[384]{0:T(512)} %copy-done.32) | copy-start | bytes 4612
  191.0 55.1 %copy-start.37 = (f32[2048]{0:T(1024)S(1)}, f32[2048]{0:T(1024)}, u32[]{:S(2)}) copy-start(f32[2048]{0:T(1024)} %param.31) | copy-start | bytes 24580
  255.0 7.3 %copy-start.5 = (bf16[384,1024]{1,0:T(8,128)(2,1)S(1)}, bf16[384,1024]{1,0:T(8,128)(2,1)}, u32[]{:S(2)}) copy-start(bf16[384,1024]{1,0:T(8,128)(2,1)} %param.17) | copy-start | bytes 2359300
  255.0 20.9 %all-gather.17.cloned.1.call-start = ((), (), s32[]{:S(2)}) async-start(), calls=%async_computation.7 | async-start | bytes 2359296 | tf_op jit(solution)/shard_map/all_gather | solution.py:103
  264.7 139.0 %all-gather.19.cloned.1.call-start = ((), (), s32[]{:S(2)}) async-start(), calls=%async_computation.8 | async-start | bytes 9437184 | tf_op jit(solution)/shard_map/all_gather | solution.py:108
  265.4 263.1 %all-gather.21.cloned.1.call-start = ((), (), s32[]{:S(2)}) async-start(), calls=%async_computation.9 | async-start | bytes 9437184 | tf_op jit(solution)/shard_map/all_gather | solution.py:109
  266.2 137.5 %copy-start.38 = (f32[2048]{0:T(1024)S(1)}, f32[2048]{0:T(1024)}, u32[]{:S(2)}) copy-start(f32[2048]{0:T(1024)} %param.32) | copy-start | bytes 24580
  266.2 387.5 %all-gather.23.cloned.1.call-start = ((), (), s32[]{:S(2)}) async-start(), calls=%async_computation.10 | async-start | bytes 9437184 | tf_op jit(solution)/shard_map/all_gather | solution.py:118
  266.9 409.8 %reduce-scatter.5.cloned.1.call-start = ((), (), s32[]{:S(2)}) async-start(), calls=%async_computation.11 | async-start | bytes 2359296 | tf_op jit(solution)/shard_map/reduce_scatter | solution.py:120
  275.9 127.8 %copy-start.9 = (bf16[384,2048]{1,0:T(8,128)(2,1)S(1)}, bf16[384,2048]{1,0:T(8,128)(2,1)}, u32[]{:S(2)}) copy-start(bf16[384,2048]{1,0:T(8,128)(2,1)} %all-gather.17.cloned.1.call-done) | copy-start | bytes 4718596
  669.5 7.3 %copy-start.2 = (bf16[384,1024]{1,0:T(8,128)(2,1)S(1)}, bf16[384,1024]{1,0:T(8,128)(2,1)}, u32[]{:S(2)}) copy-start(bf16[384,1024]{1,0:T(8,128)(2,1)} %add_convert_fusion) | copy-start | bytes 2359300
  669.5 11.3 %dynamic-slice-start = ((f32[2048]{0:T(1024)}, s32[]{:T(128)}), f32[1024]{0:T(1024)S(1)}, s32[]{:S(2)}) async-start(f32[2048]{0:T(1024)} %param.33, s32[]{:T(128)} %select_n.8), calls=%async_computation.12 | async-start | bytes 8704 | tf_op jit(solution)/shard_map/dynamic_slice | solution.py:130
  676.8 4.0 copy-start.6
  676.8 5.2 copy-start.1
  (18 other events, 32.0 us)
Sparse Core Ops, SparseCore 0:
  8.9 12.5 all-gather.8
  23.6 73.9 all-gather.10
  99.7 71.3 all-gather.12
  172.9 73.1 all-gather.14
  255.1 7.1 reduce-scatter.2
  264.8 11.0 all-gather.16
  278.0 125.6 all-gather.18
  405.8 122.6 all-gather.20
  530.6 123.1 all-gather.22
  669.6 7.1 reduce-scatter.4
where the time goes:
time: 690 us; the launch traced here: 689 us
  waiting for transfers between devices  527 us (76%)
  local copies, waits for them, and re-layouts  70.5 us (10%)
  matrix products  47.9 us (7%)
  other arithmetic  26.7 us (4%)
  between operations  14.2 us (2%)
    all_gather x1, waiting for transfers between devices, shards(): lax.all_gather(feedforward_gate_upward, 'fs', axis=0, tiled=True)  126 us
    all_gather x1, waiting for transfers between devices, shards(): lax.all_gather(feedforward_down_weight, 'fs', axis=1, tiled=True)  117 us
    all_gather x1, waiting for transfers between devices, shards(): lax.all_gather(feedforward_value_upward, 'fs', axis=0, tiled=True)  116 us
    all_gather x1, waiting for transfers between devices, shards(): lax.all_gather(recurrence_input_weight, 'fs', axis=0, tiled=True)  74.2 us
    slice x49, local copies, waits for them, and re-layouts, shards(): states = lax.associative_scan(chain_step, (decay_rate, inflow), axis=0)[1]  56.5 us
    all_gather x1, waiting for transfers between devices, shards(): lax.all_gather(recurrence_output_weight, 'fs', axis=1, tiled=True)  53.4 us
    dot_general x2, matrix products, project_with(): jnp.dot(left_rows, weight_piece, preferred_element_type=jnp.float32)  24.6 us
  transfers between devices with their start and end apart: 10, of which 9 were waited for; matrix products, arithmetic and copies ran while one was open for 17% of the time, Pallas kernels for 0%

commit v1 on v0

--- a/solution.py
+++ b/solution.py
@@ -1,6 +1,10 @@
+import functools
+
 import jax
 import jax.numpy as jnp
 from jax import lax
+from jax.experimental import pallas as pl
+from jax.experimental.pallas import tpu as pltpu
 from jax.sharding import PartitionSpec as P
 
 EPS = 1e-06
@@ -38,7 +42,155 @@
     return jnp.dot(left_rows, weight_piece, preferred_element_type=jnp.float32).astype(jnp.bfloat16)
 
 
+def third_rows(rows):
+    return rows // 3 // 16 * 16
+
+
+class RingGather:
+    def __init__(self, n, sources, targets, send_sems, recv_sems):
+        self.n = n
+        self.sources = sources
+        self.targets = targets
+        self.send_sems = send_sems
+        self.recv_sems = recv_sems
+        self.rep = lax.axis_index("rep")
+        fs = lax.axis_index("fs")
+        self.fs = fs
+        side = lax.rem(fs, 2)
+        depth = fs // 2
+        self.place = depth + side * (n - 1 - 2 * depth)
+
+    def member(self, shift):
+        place = lax.rem(self.place + shift + 2 * self.n, self.n)
+        side = place // (self.n // 2)
+        depth = place + side * (self.n - 1 - 2 * place)
+        return 2 * depth + side
+
+    def neighbours(self):
+        return (
+            {"fs": self.member(1)},
+            {"fs": self.member(-1)},
+            {"rep": 1 - self.rep},
+            {"tp": 1 - lax.axis_index("tp")},
+        )
+
+    def enter(self):
+        barrier = pltpu.get_barrier_semaphore()
+        for device in self.neighbours():
+            pl.semaphore_signal(
+                barrier, inc=1, device_id=device, device_id_type=pl.DeviceIdType.MESH
+            )
+        pl.semaphore_wait(barrier, 4)
+
+    def piece(self, ref, w, lane, base, other=False):
+        rows = self.sources[w].shape[0]
+        part = third_rows(rows)
+        if lane == 1:
+            return ref.at[pl.ds(pl.multiple_of(base + part, 16), rows - 2 * part), :]
+        rep = 1 - self.rep if other else self.rep
+        return ref.at[pl.ds(pl.multiple_of(base + rep * (rows - part), 16), part), :]
+
+    def heading(self, w, lane):
+        return 1 if (w + lane) % 2 == 0 else -1
+
+    def copy(self, w, lane, step, source, target, device):
+        return pltpu.make_async_remote_copy(
+            src_ref=source,
+            dst_ref=target,
+            send_sem=self.send_sems.at[w, lane, step],
+            recv_sem=self.recv_sems.at[w, lane, step],
+            device_id=device,
+            device_id_type=pl.DeviceIdType.MESH,
+        )
+
+    def hop(self, w, lane, step):
+        way = self.heading(w, lane)
+        base = self.member(-way * step) * self.sources[w].shape[0]
+        target = self.piece(self.targets[w], w, lane, base)
+        source = self.piece(self.sources[w], w, lane, 0) if step == 0 else target
+        return self.copy(w, lane, step, source, target, {"fs": self.member(way)})
+
+    def arrival(self, w, lane, step):
+        way = self.heading(w, lane)
+        base = self.member(-way * (step + 1)) * self.sources[w].shape[0]
+        target = self.piece(self.targets[w], w, lane, base)
+        return self.copy(w, lane, step, target, target, {"fs": self.member(way)})
+
+    def cross(self, w, step, other=False):
+        way = self.heading(w, 0)
+        if other:
+            way_base = self.member(-way * (step + 1)) * self.sources[w].shape[0]
+            target = self.piece(self.targets[w], w, 0, way_base, other=True)
+        else:
+            way_base = self.member(-way * (step + 1)) * self.sources[w].shape[0]
+            target = self.piece(self.targets[w], w, 0, way_base)
+        return self.copy(w, 2, step, target, target, {"rep": 1 - self.rep})
+
+    def local(self, w, sem):
+        rows = self.sources[w].shape[0]
+        own = self.targets[w].at[pl.ds(pl.multiple_of(self.fs * rows, 16), rows), :]
+        return pltpu.make_async_copy(self.sources[w], own, sem.at[w])
+
+    def start(self, w):
+        for lane in (0, 1):
+            self.hop(w, lane, 0).start()
+
+    def serve(self, w, step):
+        for lane in (0, 1):
+            self.arrival(w, lane, step).wait_recv()
+            if step + 1 < self.n - 1:
+                self.hop(w, lane, step + 1).start()
+            if lane == 0:
+                self.cross(w, step).start()
+
+    def crossed(self, w):
+        for step in range(self.n - 1):
+            self.cross(w, step, other=True).wait_recv()
+
+    def drain(self, w):
+        for step in range(self.n - 1):
+            self.hop(w, 0, step).wait_send()
+            self.hop(w, 1, step).wait_send()
+            self.cross(w, step).wait_send()
+
+
+def gather_kernel(n, *refs):
+    sources, targets = refs[:6], refs[6:12]
+    local_sems, send_sems, recv_sems = refs[12:]
+    ring = RingGather(n, sources, targets, send_sems, recv_sems)
+    ring.enter()
+    for w in range(6):
+        ring.local(w, local_sems).start()
+    groups = ((0, 1, 2), (3, 4, 5))
+    for group in groups:
+        for w in group:
+            ring.start(w)
+        for step in range(n - 1):
+            for w in group:
+                ring.serve(w, step)
+    for w in range(6):
+        ring.local(w, local_sems).wait()
+        ring.crossed(w)
+        ring.drain(w)
+
+
+def gather_weights(n, weights):
+    return pl.pallas_call(
+        functools.partial(gather_kernel, n),
+        out_shape=[jax.ShapeDtypeStruct((n * w.shape[0], w.shape[1]), w.dtype) for w in weights],
+        in_specs=[pl.BlockSpec(memory_space=pl.ANY)] * 6,
+        out_specs=[pl.BlockSpec(memory_space=pl.ANY)] * 6,
+        scratch_shapes=[
+            pltpu.SemaphoreType.DMA((6,)),
+            pltpu.SemaphoreType.DMA((6, 3, n - 1)),
+            pltpu.SemaphoreType.DMA((6, 3, n - 1)),
+        ],
+        compiler_params=pltpu.CompilerParams(collective_id=0, has_side_effects=True),
+    )(*weights)
+
+
 def shards(
+    ringed,
     stream,
     recurrence_input_weight,
     output_gate_weight,
@@ -58,6 +210,31 @@
     closing_norm_gain,
 ):
     tok_rows = stream.shape[0]
+    fs_size = lax.axis_size("fs")
+    if ringed:
+        weights = list(gather_weights(
+            fs_size,
+            (
+                recurrence_input_weight,
+                output_gate_weight,
+                recurrence_output_weight,
+                feedforward_gate_upward,
+                feedforward_value_upward,
+                feedforward_down_weight,
+            ),
+        ))
+        for w in (2, 5):
+            stacked = weights[w].reshape(fs_size, -1, weights[w].shape[1])
+            weights[w] = jnp.concatenate([stacked[f] for f in range(fs_size)], axis=1)
+    else:
+        weights = [
+            lax.all_gather(recurrence_input_weight, "fs", axis=0, tiled=True),
+            lax.all_gather(output_gate_weight, "fs", axis=0, tiled=True),
+            lax.all_gather(recurrence_output_weight, "fs", axis=1, tiled=True),
+            lax.all_gather(feedforward_gate_upward, "fs", axis=0, tiled=True),
+            lax.all_gather(feedforward_value_upward, "fs", axis=0, tiled=True),
+            lax.all_gather(feedforward_down_weight, "fs", axis=1, tiled=True),
+        ]
     head_count = recurrence_gate_matrix.shape[0]
     block_size = recurrence_gate_matrix.shape[1]
     whole_rows = lax.all_gather(stream, "tp", axis=1, tiled=True)
@@ -65,8 +242,8 @@
     rec_sum, gate_sum = fold_pair(
         normed,
         (
-            lax.all_gather(recurrence_input_weight, "fs", axis=0, tiled=True),
-            lax.all_gather(output_gate_weight, "fs", axis=0, tiled=True),
+            weights[0],
+            weights[1],
         ),
     )
     rec_in = rec_sum.astype(jnp.bfloat16)
@@ -91,7 +268,7 @@
         * jax.nn.gelu(gate_src.astype(jnp.float32))
     ).astype(jnp.bfloat16)
     mix_terms = project_with(
-        mixed_out, lax.all_gather(recurrence_output_weight, "fs", axis=1, tiled=True)
+        mixed_out, weights[2]
     )
     branch = lax.psum_scatter(
         lax.optimization_barrier(mix_terms).astype(jnp.float32).astype(jnp.bfloat16),
@@ -105,8 +282,8 @@
     gate_sum_ffn, value_sum_ffn = fold_pair(
         normed_ffn,
         (
-            lax.all_gather(feedforward_gate_upward, "fs", axis=0, tiled=True),
-            lax.all_gather(feedforward_value_upward, "fs", axis=0, tiled=True),
+            weights[3],
+            weights[4],
         ),
     )
     gate_up = gate_sum_ffn.astype(jnp.bfloat16)
@@ -115,7 +292,7 @@
     value_conv = causal_mix(value_up.astype(jnp.float32), feedforward_value_taps)
     hidden = (jax.nn.gelu(gate_conv) * value_conv).astype(jnp.bfloat16)
     down_terms = project_with(
-        hidden, lax.all_gather(feedforward_down_weight, "fs", axis=1, tiled=True)
+        hidden, weights[5]
     )
     branch_ffn = lax.psum_scatter(
         lax.optimization_barrier(down_terms).astype(jnp.float32).astype(jnp.bfloat16),
@@ -154,4 +331,6 @@
         P(),
     )
     out_specs = P(("rep", "fs"), "tp")
-    return jax.shard_map(shards, mesh=mesh, in_specs=in_specs, out_specs=out_specs, check_vma=False)
+    ringed = mesh.shape["rep"] == 2 and mesh.shape["tp"] == 2 and mesh.shape["fs"] == 8
+    body = functools.partial(shards, ringed)
+    return jax.shard_map(body, mesh=mesh, in_specs=in_specs, out_specs=out_specs, check_vma=False)

time: 690 us -> 462 us (0.67)
  waiting for transfers between devices: 527 us -> 14.1 us
  Pallas kernels: 0 us -> 260 us
  local copies, waits for them, and re-layouts: 70.5 us -> 102 us
  matrix products: 47.9 us -> 39.8 us
    all_gather x6 -> x0, waiting for transfers between devices: 487 us -> none  [the longest x1 126 us: shards(): lax.all_gather(feedforward_gate_upward, 'fs', axis=0, tiled=True)]
    pallas_call x0 -> x1, Pallas kernels: none -> 260 us  [gather_weights(): pl.pallas_call(functools.partial(gather_kernel, n), out_shape=[jax.ShapeD...]
    unnamed x78 -> x84, local copies, waits for them, and re-layouts: 1.55 us -> 27.2 us
    all_gather x1, waiting for transfers between devices: 12 us -> 0.01 us  [shards(): whole_rows = lax.all_gather(stream, 'tp', axis=1, tiled=True)]
    reduce_scatter x1, waiting for transfers between devices: 7.06 us -> 0.01 us  [shards(): lax.psum_scatter(lax.optimization_barrier(mix_terms).astype(jnp.float32)....]
  transfers between devices with their start and end apart: 10 -> 4, of which waited for: 9 -> 2; matrix products, arithmetic and copies ran while one was open for 17% -> 7% of each run, Pallas kernels for 0% -> 56%
where the time goes in v1:
time: 462 us; the launch traced here: 460 us
  Pallas kernels  260 us (56%)
  local copies, waits for them, and re-layouts  102 us (22%)
  matrix products  39.8 us (9%)
  other arithmetic  28.3 us (6%)
  waiting for transfers between devices  14.1 us (3%)
  between operations  13.8 us (3%)
    pallas_call x1, Pallas kernels, gather_weights(): pl.pallas_call(functools.partial(gather_kernel, n), out_shape=[jax.ShapeD...  260 us
    slice x49, local copies, waits for them, and re-layouts, shards(): states = lax.associative_scan(chain_step, (decay_rate, inflow), axis=0)[1]  58 us
    unnamed x84, local copies, waits for them, and re-layouts  27.2 us
    dot_general x2, matrix products, project_with(): jnp.dot(left_rows, weight_piece, preferred_element_type=jnp.float32)  19.2 us
    dot_general x2, matrix products, fold_pair(): jnp.dot(source, pieces[0], preferred_element_type=jnp.float32)  12.2 us
    mul x7, other arithmetic, chain_step(): return (earlier[0] * following[0], following[0] * earlier[1] + following[1])  11 us
    reduce_scatter x1, waiting for transfers between devices, shards(): lax.psum_scatter(lax.optimization_barrier(down_terms).astype(jnp.float32)...  10.3 us
  transfers between devices with their start and end apart: 4, of which 2 were waited for; matrix products, arithmetic and copies ran while one was open for 7% of the time, Pallas kernels for 56%

profile of v1, /device:TPU:0, one launch (start us, length us, event | category | flops | bytes accessed | tf_op | source)
XLA Modules:
  0.0 460.2 jit_solution(5831783644481091178)
XLA Ops:
  8.2 259.9 %shard_map.163 = (bf16[2048,1024]{1,0:T(8,128)(2,1)}, bf16[2048,1024]{1,0:T(8,128)(2,1)}, bf16[8192,256]{1,0:T(8,128)(2,1)}, bf16[2048,2048]{1,0:T(8,128)(2,1)},...) custom-call(bf16[256,1024]{1,0:T(8,128)(2,1)} %refs_0_.1, bf16[256,1024]{1,0:T(8,128)(2,1)} %refs_1_.1, ...), custom_call_target="tpu_custom_call" | custom-call | tf_op jit(solution)/shard_map/pallas_call | solution.py:178
  268.1 2.1 slice_dynamic-update-slice_fusion.15
  270.2 1.9 slice_dynamic-update-slice_fusion.14
  272.1 2.0 slice_dynamic-update-slice_fusion.13
  274.1 1.9 slice_dynamic-update-slice_fusion.12
  279.5 1.8 fusion
  281.3 4.5 fusion.36
  295.5 2.0 fusion.67
  303.4 2.3 fusion.68
  312.4 1.9 fusion.69
  354.2 3.5 slice.315
  362.8 3.8 pad.76
  369.1 3.8 pad.75
  374.3 2.0 copy.24
  378.0 8.9 %convolution_convert_fusion.3 = bf16[384,2048]{1,0:T(8,128)(2,1)} fusion(bf16[1024,2048]{1,0:T(8,128)(2,1)} %slice_dynamic-update-slice_fusion.8, f32[384,1024]{1,0:T(8,128)} %copy.25, bf16[2048,1024]{1,0:T(8,128)(2,1)} %get-tuple-element.12, bf16[384,2048]{1,0:T(8,128)(2,1)S(1)} %copy-done.6, f32[2048]{0:T(1024)S(1)} %copy-done.33, f32[384]{0:T(512)S(1)} %copy-done.29), kind=kOutput, calls=%fused_computation.23 | convolution fusion | flops 3229876224 | bytes 13116928 | tf_op jit(solution)/shard_map/dot_general | solution.py:42
  387.0 2.4 slice_dynamic-update-slice_fusion.7
  389.3 2.3 slice_dynamic-update-slice_fusion.6
  391.6 2.4 slice_dynamic-update-slice_fusion.5
  394.1 2.4 slice_dynamic-update-slice_fusion.4
  396.5 2.3 slice_dynamic-update-slice_fusion.3
  398.8 2.3 add_convert_fusion
  401.2 2.4 slice_dynamic-update-slice_fusion.2
  403.6 2.4 slice_dynamic-update-slice_fusion.1
  406.0 2.3 slice_dynamic-update-slice_fusion
  408.3 3.1 all-gather.5.cloned.1.call-done
  411.4 1.8 fusion.3
  413.2 7.7 %fusion.15 = f32[384,2048]{1,0:T(8,128)S(1)} fusion(bf16[2048,2048]{1,0:T(8,128)(2,1)} %get-tuple-element.14, bf16[384,2048]{1,0:T(8,128)(2,1)} %all-gather.5.cloned.1.call-done, f32[2048]{0:T(1024)S(1)} %copy-done.34, f32[384]{0:T(512)S(1)} %add_rsqrt_fusion.1), kind=kOutput, calls=%fused_computation.24 | convolution fusion | flops 3225944064 | bytes 13116928 | tf_op jit(solution)/shard_map/dot_general | solution.py:36
  420.9 5.9 %fusion.16 = f32[384,2048]{1,0:T(8,128)S(1)} fusion(bf16[2048,2048]{1,0:T(8,128)(2,1)} %get-tuple-element.15, bf16[384,2048]{1,0:T(8,128)(2,1)S(1)} %copy-done.7, f32[2048]{0:T(1024)S(1)} %copy-done.34, f32[384]{0:T(512)S(1)} %add_rsqrt_fusion.1), kind=kOutput, calls=%fused_computation.25 | convolution fusion | flops 3225944064 | bytes 13116928 | tf_op jit(solution)/shard_map/dot_general | solution.py:37
  426.8 10.3 %convolution_convert_fusion = bf16[384,2048]{1,0:T(8,128)(2,1)} fusion(bf16[2048,2048]{1,0:T(8,128)(2,1)} %slice_dynamic-update-slice_fusion, f32[384,2048]{1,0:T(8,128)S(1)} %fusion.16, f32[384,2048]{1,0:T(8,128)S(1)} %fusion.15, f32[2048]{0:T(1024)S(1)} %bitcast.45, f32[2048]{0:T(1024)S(1)} %bitcast.46, f32[2048]{0:T(1024)S(1)} %bitcast.44, ...), kind=kOutput, calls=%fused_computation.20 | convolution fusion | flops 3237740544 | bytes 16302080 | tf_op jit(solution)/shard_map/dot_general | solution.py:42
  437.1 10.3 %reduce-scatter.5.cloned.1.call-done = bf16[384,1024]{1,0:T(8,128)(2,1)} async-done(((bf16[384,2048]{1,0:T(8,128)(2,1)}), bf16[384,1024]{1,0:T(8,128)(2,1)}) %reduce-scatter.5.cloned.1.call-update) | async-done | bytes 786448 | tf_op jit(solution)/shard_map/reduce_scatter | solution.py:297
  448.9 2.5 psum.7
  451.3 2.3 multiply_convert_fusion
  (186 shorter events, 79.0 us)
Async XLA Ops:
  6.5 280.1 %copy-start = (bf16[8,128,128]{2,1,0:T(8,128)(2,1)S(1)}, bf16[8,128,128]{2,1,0:T(8,128)(2,1)}, u32[]{:S(2)}) copy-start(bf16[8,128,128]{2,1,0:T(8,128)(2,1)} %param.20) | copy-start | bytes 786436
  6.5 273.0 %all-gather.3.cloned.1.call-start = ((), (), s32[]{:S(2)}) async-start(), calls=%async_computation.2 | async-start | bytes 2359296 | tf_op jit(solution)/shard_map/all_gather | solution.py:240
  7.3 391.5 %reduce-scatter.3.cloned.1.call-start = ((), (), s32[]{:S(2)}) async-start(), calls=%async_computation.3 | async-start | bytes 2359296 | tf_op jit(solution)/shard_map/reduce_scatter | solution.py:273
  8.2 263.9 %copy-start.26 = (f32[1024]{0:T(1024)S(1)}, f32[1024]{0:T(1024)}, u32[]{:S(2)}) copy-start(f32[1024]{0:T(1024)} %param.22) | copy-start | bytes 12292
  268.1 7.9 %copy-start.3 = (bf16[8192,256]{1,0:T(8,128)(2,1)S(1)}, bf16[8192,256]{1,0:T(8,128)(2,1)}, u32[]{:S(2)}) copy-start(bf16[8192,256]{1,0:T(8,128)(2,1)} %get-tuple-element.13) | copy-start | bytes 12582916
  276.0 5.3 %copy-start.32 = (f32[2048]{0:T(1024)S(1)}, f32[2048]{0:T(1024)}, u32[]{:S(2)}) copy-start(f32[2048]{0:T(1024)} %param.31) | copy-start | bytes 24580
  281.3 4.5 copy-start.28
  281.3 5.3 %copy-start.31 = (f32[384,8]{0,1:T(8,128)S(1)}, f32[384,8]{0,1:T(8,128)}, u32[]{:S(2)}) copy-start(f32[384,8]{0,1:T(8,128)} %param.24) | copy-start | bytes 36868
  287.8 6.1 %copy-start.4 = (f32[384,8,128]{2,0,1:T(8,128)}, f32[384,8,128]{2,0,1:T(8,128)S(1)}, u32[]{:S(2)}) copy-start(f32[384,8,128]{2,0,1:T(8,128)S(1)} %get-tuple-element.44) | copy-start | bytes 4718596
  340.0 18.3 %copy-start.14 = (f32[3,8,128]{2,0,1:T(4,128)S(1)}, f32[3,8,128]{2,0,1:T(4,128)}, u32[]{:S(2)}) copy-start(f32[3,8,128]{2,0,1:T(4,128)} %slice.354) | copy-start | bytes 36868
  340.0 18.3 %copy-start.15 = (f32[3,8,128]{2,0,1:T(4,128)S(1)}, f32[3,8,128]{2,0,1:T(4,128)}, u32[]{:S(2)}) copy-start(f32[3,8,128]{2,0,1:T(4,128)} %slice.352) | copy-start | bytes 36868
  343.7 15.0 %copy-start.13 = (f32[5,8,128]{2,0,1:T(8,128)S(1)}, f32[5,8,128]{2,0,1:T(8,128)}, u32[]{:S(2)}) copy-start(f32[5,8,128]{2,0,1:T(8,128)} %slice.364) | copy-start | bytes 61444
  345.0 13.3 %copy-start.16 = (f32[3,8,128]{2,0,1:T(4,128)S(1)}, f32[3,8,128]{2,0,1:T(4,128)}, u32[]{:S(2)}) copy-start(f32[3,8,128]{2,0,1:T(4,128)} %slice.356) | copy-start | bytes 36868
  345.0 13.5 %copy-start.17 = (f32[2,8,128]{2,0,1:T(2,128)S(1)}, f32[2,8,128]{2,0,1:T(2,128)}, u32[]{:S(2)}) copy-start(f32[2,8,128]{2,0,1:T(2,128)} %slice.351) | copy-start | bytes 24580
  345.0 13.6 %copy-start.18 = (f32[2,8,128]{2,0,1:T(2,128)S(1)}, f32[2,8,128]{2,0,1:T(2,128)}, u32[]{:S(2)}) copy-start(f32[2,8,128]{2,0,1:T(2,128)} %slice.362) | copy-start | bytes 24580
  345.0 13.6 %copy-start.25 = (f32[1,8,128]{2,0,1:T(1,128)S(1)}, f32[1,8,128]{2,0,1:T(1,128)}, u32[]{:S(2)}) copy-start(f32[1,8,128]{2,0,1:T(1,128)} %slice.407) | copy-start | bytes 12292
  345.0 13.7 %copy-start.24 = (f32[1,8,128]{2,0,1:T(1,128)S(1)}, f32[1,8,128]{2,0,1:T(1,128)}, u32[]{:S(2)}) copy-start(f32[1,8,128]{2,0,1:T(1,128)} %slice.406) | copy-start | bytes 12292
  352.6 8.1 %copy-start.12 = (f32[23,8,128]{2,0,1:T(8,128)S(1)}, f32[23,8,128]{2,0,1:T(8,128)}, u32[]{:S(2)}) copy-start(f32[23,8,128]{2,0,1:T(8,128)} %slice.368) | copy-start | bytes 282628
  352.6 8.1 %copy-start.23 = (f32[1,8,128]{2,0,1:T(1,128)S(1)}, f32[1,8,128]{2,0,1:T(1,128)}, u32[]{:S(2)}) copy-start(f32[1,8,128]{2,0,1:T(1,128)} %slice.404) | copy-start | bytes 12292
  354.2 6.9 %copy-start.10 = (f32[47,8,128]{2,0,1:T(8,128)S(1)}, f32[47,8,128]{2,0,1:T(8,128)}, u32[]{:S(2)}) copy-start(f32[47,8,128]{2,0,1:T(8,128)} %slice.327) | copy-start | bytes 577540
  354.2 6.9 %copy-start.11 = (f32[47,8,128]{2,0,1:T(8,128)S(1)}, f32[47,8,128]{2,0,1:T(8,128)}, u32[]{:S(2)}) copy-start(f32[47,8,128]{2,0,1:T(8,128)} %slice.370) | copy-start | bytes 577540
  362.8 5.4 %copy-start.21 = (f32[1,8,128]{2,0,1:T(1,128)S(1)}, f32[1,8,128]{2,0,1:T(1,128)}, u32[]{:S(2)}) copy-start(f32[1,8,128]{2,0,1:T(1,128)} %slice.401) | copy-start | bytes 12292
  378.0 9.0 %copy-start.19 = (f32[3,2048]{1,0:T(4,128)S(1)}, f32[3,2048]{1,0:T(4,128)}, u32[]{:S(2)}) copy-start(f32[3,2048]{1,0:T(4,128)} %param.28) | copy-start | bytes 73732
  386.9 24.5 %all-gather.5.cloned.1.call-start = ((), (), s32[]{:S(2)}) async-start(), calls=%async_computation.4 | async-start | bytes 2359296 | tf_op jit(solution)/shard_map/all_gather | solution.py:280
  391.6 7.2 %copy-start.5 = (bf16[384,1024]{1,0:T(8,128)(2,1)S(1)}, bf16[384,1024]{1,0:T(8,128)(2,1)}, u32[]{:S(2)}) copy-start(bf16[384,1024]{1,0:T(8,128)(2,1)} %param.17) | copy-start | bytes 2359300
  396.5 4.7 %copy-start.20 = (f32[3,2048]{1,0:T(4,128)S(1)}, f32[3,2048]{1,0:T(4,128)}, u32[]{:S(2)}) copy-start(f32[3,2048]{1,0:T(4,128)} %param.29) | copy-start | bytes 73732
  401.1 46.3 %reduce-scatter.5.cloned.1.call-start = ((), (), s32[]{:S(2)}) async-start(), calls=%async_computation.5 | async-start | bytes 2359296 | tf_op jit(solution)/shard_map/reduce_scatter | solution.py:297
  403.6 9.6 %copy-start.34 = (f32[2048]{0:T(1024)S(1)}, f32[2048]{0:T(1024)}, u32[]{:S(2)}) copy-start(f32[2048]{0:T(1024)} %param.32) | copy-start | bytes 24580
  413.2 7.7 %copy-start.7 = (bf16[384,2048]{1,0:T(8,128)(2,1)S(1)}, bf16[384,2048]{1,0:T(8,128)(2,1)}, u32[]{:S(2)}) copy-start(bf16[384,2048]{1,0:T(8,128)(2,1)} %all-gather.5.cloned.1.call-done) | copy-start | bytes 4718596
  426.8 10.3 %copy-start.27 = (f32[2048]{0:T(1024)S(1)}, f32[2048]{0:T(1024)}, u32[]{:S(2)}) copy-start(f32[2048]{0:T(1024)} %param.33) | copy-start | bytes 24580
  426.8 20.6 %copy-start.2 = (bf16[384,1024]{1,0:T(8,128)(2,1)S(1)}, bf16[384,1024]{1,0:T(8,128)(2,1)}, u32[]{:S(2)}) copy-start(bf16[384,1024]{1,0:T(8,128)(2,1)} %add_convert_fusion) | copy-start | bytes 2359300
  426.8 26.8 %copy-start.1 = (bf16[8,128,128]{2,1,0:T(8,128)(2,1)S(1)}, bf16[8,128,128]{2,1,0:T(8,128)(2,1)}, u32[]{:S(2)}) copy-start(bf16[8,128,128]{2,1,0:T(8,128)(2,1)} %param.20) | copy-start | bytes 786436
  (7 other events, 18.6 us)
Sparse Core Ops, SparseCore 0:
  8.9 12.5 all-gather.2
  387.0 9.1 reduce-scatter.2
  401.3 10.0 all-gather.4
  437.2 10.1 reduce-scatter.4

commit v2 on v1

--- a/solution.py
+++ b/solution.py
@@ -154,39 +154,255 @@
             self.cross(w, step).wait_send()
 
 
-def gather_kernel(n, *refs):
-    sources, targets = refs[:6], refs[6:12]
-    local_sems, send_sems, recv_sems = refs[12:]
+def gelu_of(x):
+    return 0.5 * x * (1.0 + jnp.tanh(0.7978845608028654 * (x + 0.044715 * (x * x * x))))
+
+
+def one_less_exp(z):
+    series = 1.0 + z * (1.0 / 6.0)
+    for order in (5.0, 4.0, 3.0, 2.0):
+        series = 1.0 + z * (1.0 / order) * series
+    return jnp.where(z > -0.35, -z * series, 1.0 - jnp.exp(z))
+
+
+def tap_rows(values, taps_ref, cols):
+    extent = taps_ref.shape[0]
+    summed = taps_ref[extent - 1 : extent, cols] * values
+    row = lax.broadcasted_iota(jnp.int32, values.shape, 0)
+    for back in range(1, extent):
+        moved = jnp.where(row >= back, pltpu.roll(values, back, 0), 0.0)
+        summed = summed + taps_ref[extent - 1 - back : extent - back, cols] * moved
+    return summed
+
+
+def dot32(a, b):
+    return jnp.dot(a, b, preferred_element_type=jnp.float32)
+
+
+def layer_kernel(n, *refs):
+    sources = refs[:6]
+    (stream, reset_map, admit_map, decay_base, taps, spike) = refs[6:12]
+    (gate_taps, value_taps, rec_gain, ffn_gain, last_gain, out) = refs[12:18]
+    targets = refs[18:24]
+    (stream_in, normed, gate_src, decay, inflow, mixed) = refs[24:30]
+    (away, landed, kept, middle, middle_in, hidden, final, sums, sums_in) = refs[30:39]
+    local_sems, send_sems, recv_sems, pair_send, pair_recv = refs[39:]
+    tokens, width = stream.shape
+    me = lax.axis_index("tp")
     ring = RingGather(n, sources, targets, send_sems, recv_sems)
+    bf16, f32 = jnp.bfloat16, jnp.float32
+    tile = 256
+    strip = 48
+
+    def pair(i, source, target):
+        return pltpu.make_async_remote_copy(
+            src_ref=source,
+            dst_ref=target,
+            send_sem=pair_send.at[i],
+            recv_sem=pair_recv.at[i],
+            device_id={"tp": 1 - me},
+            device_id_type=pl.DeviceIdType.MESH,
+        )
+
+    def half(which):
+        return pl.ds(pl.multiple_of(which * width, 128), width)
+
+    def strips(body):
+        def step(i, carry):
+            body(pl.ds(pl.multiple_of(i * strip, 16), strip))
+            return carry
+
+        lax.fori_loop(0, tokens // strip, step, 0)
+
+    def norm_into(mine, theirs, gain):
+        def body(rows):
+            a = mine[rows, :].astype(f32)
+            b = theirs[rows, :].astype(f32)
+            total = jnp.sum(a * a, axis=1, keepdims=True) + jnp.sum(b * b, axis=1, keepdims=True)
+            inverse = lax.rsqrt(total * (1.0 / (2 * width)) + EPS)
+            normed[rows, half(me)] = (a * inverse * gain[:, half(me)]).astype(bf16)
+            normed[rows, half(1 - me)] = (b * inverse * gain[:, half(1 - me)]).astype(bf16)
+
+        strips(body)
+
+    def project(i, rows, w):
+        depth = rows.shape[1]
+        per_half = n // 2
+
+        def into(target, which):
+            def step(j, carry):
+                slot = which * per_half + j
+                block = targets[w][pl.ds(pl.multiple_of(slot * depth, 16), depth), :]
+                cols = pl.ds(pl.multiple_of(j * tile, 128), tile)
+                target[:, cols] = dot32(rows[...], block).astype(bf16)
+                return carry
+
+            lax.fori_loop(0, per_half, step, 0)
+
+        into(away.at[i], 1 - me)
+        sent = pair(1 + i, away.at[i], landed.at[i])
+        sent.start()
+        into(kept, me)
+        sent.wait()
+
+    def ready(w):
+        ring.local(w, local_sems).wait()
+        ring.crossed(w)
+
     ring.enter()
+    first = pair(0, stream, stream_in)
+    first.start()
+    for w in range(3):
+        ring.start(w)
     for w in range(6):
         ring.local(w, local_sems).start()
-    groups = ((0, 1, 2), (3, 4, 5))
-    for group in groups:
-        for w in group:
-            ring.start(w)
-        for step in range(n - 1):
-            for w in group:
-                ring.serve(w, step)
+    first.wait()
+    norm_into(stream, stream_in, rec_gain)
+    for step in range(n - 1):
+        for w in range(3):
+            ring.serve(w, step)
+        if step == n - 3:
+            ring.start(3)
+            ring.start(4)
+    for w in range(3):
+        ready(w)
+
+    def ticks(step):
+        ring.serve(3, step)
+        ring.serve(4, step)
+
+    for c in range(width // tile):
+        cols = slice(c * tile, (c + 1) * tile)
+        rec = dot32(normed[...], targets[0][:, cols]).astype(bf16).astype(f32)
+        conv = tap_rows(rec, taps, cols).astype(bf16)
+        gate_src[:, cols] = dot32(normed[...], targets[1][:, cols]).astype(bf16)
+        for part in range(tile // 128):
+            h = c * (tile // 128) + part
+            lanes = slice(h * 128, (h + 1) * 128)
+            block = conv[:, part * 128 : (part + 1) * 128]
+            reset = jax.nn.sigmoid(dot32(block, reset_map[h]))
+            admit = jax.nn.sigmoid(dot32(block, admit_map[h]))
+            log_decay = spike[:, h : h + 1] - reset * decay_base[:, lanes]
+            decay[:, lanes] = jnp.exp(log_decay)
+            inflow[:, lanes] = jnp.sqrt(one_less_exp(2.0 * log_decay)) * admit * block.astype(f32)
+        ticks(c)
+
+    row = lax.broadcasted_iota(jnp.int32, (8, width), 0)
+
+    def scan_step(i, carry):
+        rows = pl.ds(pl.multiple_of(i * 16, 16), 16)
+        a16, b16 = decay[rows, :], inflow[rows, :]
+        found = []
+        for part in range(2):
+            a, b = a16[part * 8 : part * 8 + 8], b16[part * 8 : part * 8 + 8]
+            for back in (1, 2, 4):
+                a_before = jnp.where(row >= back, pltpu.roll(a, back, 0), 1.0)
+                b_before = jnp.where(row >= back, pltpu.roll(b, back, 0), 0.0)
+                b = a * b_before + b
+                a = a * a_before
+            states = a * carry + b
+            carry = states[7:8, :]
+            found.append(states)
+        states = jnp.concatenate(found, axis=0)
+        mixed[rows, :] = (states * gelu_of(gate_src[rows, :].astype(f32))).astype(bf16)
+        return carry
+
+    lax.fori_loop(0, tokens // 16, scan_step, jnp.zeros((1, width), f32))
+    served = width // tile
+    ticks(served)
+    project(0, mixed, 2)
+
+    def add_branch(rows):
+        branch = (kept[rows, :].astype(f32) + landed[0, rows, :].astype(f32)).astype(bf16)
+        middle[rows, :] = (stream[rows, :].astype(f32) + branch.astype(f32)).astype(bf16)
+
+    strips(add_branch)
+    shared = pair(3, middle, middle_in)
+    shared.start()
+    ring.start(5)
+    shared.wait()
+    for step in range(served + 1, n - 1):
+        ticks(step)
+        if step == served + 1:
+            norm_into(middle, middle_in, ffn_gain)
+    ready(3)
+    ready(4)
+
+    def up_step(t, carry):
+        cols = pl.ds(pl.multiple_of(t * tile, 128), tile)
+        gate = dot32(normed[...], targets[3][:, cols]).astype(bf16).astype(f32)
+        gate = gelu_of(tap_rows(gate, gate_taps, cols))
+        value = dot32(normed[...], targets[4][:, cols]).astype(bf16).astype(f32)
+        hidden[:, cols] = (gate * tap_rows(value, value_taps, cols)).astype(bf16)
+        return carry
+
+    tiles = hidden.shape[1] // tile
+    for step in range(n - 1):
+        lax.fori_loop(step * tiles // (n - 1), (step + 1) * tiles // (n - 1), up_step, 0)
+        ring.serve(5, step)
+    ready(5)
+    project(1, hidden, 5)
+
+    def finish(rows):
+        branch = (kept[rows, :].astype(f32) + landed[1, rows, :].astype(f32)).astype(bf16)
+        total = middle[rows, :].astype(f32) + branch.astype(f32)
+        final[rows, :] = total
+        square = jnp.sum(total * total, axis=1, keepdims=True)
+        sums[rows, :] = jnp.broadcast_to(square, (strip, 128))
+
+    strips(finish)
+    summed = pair(4, sums, sums_in)
+    summed.start()
+    summed.wait()
+
+    def scale(rows):
+        square = sums[rows, :] + sums_in[rows, :]
+        inverse = lax.rsqrt(square * (1.0 / (2 * width)) + EPS)[:, 0:1]
+        out[rows, :] = (final[rows, :] * inverse * last_gain[:, half(me)]).astype(bf16)
+
+    strips(scale)
     for w in range(6):
-        ring.local(w, local_sems).wait()
-        ring.crossed(w)
         ring.drain(w)
 
 
-def gather_weights(n, weights):
+def fused_layer(n, weights, others):
+    tokens, width = others[0].shape
+    wide = weights[3].shape[1]
+    bf16, f32 = jnp.bfloat16, jnp.float32
+    vmem = pltpu.VMEM
     return pl.pallas_call(
-        functools.partial(gather_kernel, n),
-        out_shape=[jax.ShapeDtypeStruct((n * w.shape[0], w.shape[1]), w.dtype) for w in weights],
-        in_specs=[pl.BlockSpec(memory_space=pl.ANY)] * 6,
-        out_specs=[pl.BlockSpec(memory_space=pl.ANY)] * 6,
-        scratch_shapes=[
+        functools.partial(layer_kernel, n),
+        out_shape=jax.ShapeDtypeStruct((tokens, width), bf16),
+        in_specs=[pl.BlockSpec(memory_space=pl.ANY)] * 6
+        + [pl.BlockSpec(memory_space=vmem)] * len(others),
+        out_specs=pl.BlockSpec(memory_space=vmem),
+        scratch_shapes=[vmem((n * w.shape[0], w.shape[1]), w.dtype) for w in weights]
+        + [
+            vmem((tokens, width), bf16),
+            vmem((tokens, 2 * width), bf16),
+            vmem((tokens, width), bf16),
+            vmem((tokens, width), f32),
+            vmem((tokens, width), f32),
+            vmem((tokens, width), bf16),
+            vmem((2, tokens, width), bf16),
+            vmem((2, tokens, width), bf16),
+            vmem((tokens, width), bf16),
+            vmem((tokens, width), bf16),
+            vmem((tokens, width), bf16),
+            vmem((tokens, wide), bf16),
+            vmem((tokens, width), f32),
+            vmem((tokens, 128), f32),
+            vmem((tokens, 128), f32),
             pltpu.SemaphoreType.DMA((6,)),
             pltpu.SemaphoreType.DMA((6, 3, n - 1)),
             pltpu.SemaphoreType.DMA((6, 3, n - 1)),
+            pltpu.SemaphoreType.DMA((5,)),
+            pltpu.SemaphoreType.DMA((5,)),
         ],
-        compiler_params=pltpu.CompilerParams(collective_id=0, has_side_effects=True),
-    )(*weights)
+        compiler_params=pltpu.CompilerParams(
+            collective_id=0, has_side_effects=True, vmem_limit_bytes=66_000_000
+        ),
+    )(*weights, *others)
 
 
 def shards(
@@ -212,7 +428,7 @@
     tok_rows = stream.shape[0]
     fs_size = lax.axis_size("fs")
     if ringed:
-        weights = list(gather_weights(
+        return fused_layer(
             fs_size,
             (
                 recurrence_input_weight,
@@ -222,19 +438,28 @@
                 feedforward_value_upward,
                 feedforward_down_weight,
             ),
-        ))
-        for w in (2, 5):
-            stacked = weights[w].reshape(fs_size, -1, weights[w].shape[1])
-            weights[w] = jnp.concatenate([stacked[f] for f in range(fs_size)], axis=1)
-    else:
-        weights = [
-            lax.all_gather(recurrence_input_weight, "fs", axis=0, tiled=True),
-            lax.all_gather(output_gate_weight, "fs", axis=0, tiled=True),
-            lax.all_gather(recurrence_output_weight, "fs", axis=1, tiled=True),
-            lax.all_gather(feedforward_gate_upward, "fs", axis=0, tiled=True),
-            lax.all_gather(feedforward_value_upward, "fs", axis=0, tiled=True),
-            lax.all_gather(feedforward_down_weight, "fs", axis=1, tiled=True),
-        ]
+            (
+                stream,
+                recurrence_gate_matrix,
+                input_gate_matrix,
+                (GATE_POWER * jax.nn.softplus(-channel_decay_rate))[None, :],
+                recurrence_taps,
+                spike_log_decay,
+                feedforward_gate_taps,
+                feedforward_value_taps,
+                recurrence_norm_gain[None, :],
+                feedforward_norm_gain[None, :],
+                closing_norm_gain[None, :],
+            ),
+        )
+    weights = [
+        lax.all_gather(recurrence_input_weight, "fs", axis=0, tiled=True),
+        lax.all_gather(output_gate_weight, "fs", axis=0, tiled=True),
+        lax.all_gather(recurrence_output_weight, "fs", axis=1, tiled=True),
+        lax.all_gather(feedforward_gate_upward, "fs", axis=0, tiled=True),
+        lax.all_gather(feedforward_value_upward, "fs", axis=0, tiled=True),
+        lax.all_gather(feedforward_down_weight, "fs", axis=1, tiled=True),
+    ]
     head_count = recurrence_gate_matrix.shape[0]
     block_size = recurrence_gate_matrix.shape[1]
     whole_rows = lax.all_gather(stream, "tp", axis=1, tiled=True)

time: 462 us -> 285 us (0.62)
  local copies, waits for them, and re-layouts: 102 us -> 2.88 us
  matrix products: 39.8 us -> 0 us
  other arithmetic: 28.3 us -> 1.31 us
  Pallas kernels: 260 us -> 281 us
  waiting for transfers between devices: 14.1 us -> 0 us
  between operations: 13.8 us -> 0.01 us
    slice x52 -> x0, local copies, waits for them, and re-layouts: 58.9 us -> none  [the longest x49 58 us: shards(): states = lax.associative_scan(chain_step, (decay_rate, inflow), axis=0)[1]]
    dot_general x7 -> x0, matrix products: 39.8 us -> none  [the longest x2 19.2 us: project_with(): jnp.dot(left_rows, weight_piece, preferred_element_type=jnp.float32)]
    unnamed x84 -> x4, local copies, waits for them, and re-layouts: 27.2 us -> 2.88 us
    pallas_call x1, Pallas kernels: 260 us -> 281 us  [fused_layer(): pl.pallas_call(functools.partial(layer_kernel, n), out_shape=jax.ShapeDty...]
    reduce_scatter x2 -> x0, waiting for transfers between devices: 10.3 us -> none  [the longest x1 10.3 us: shards(): lax.psum_scatter(lax.optimization_barrier(down_terms).astype(jnp.float32)...]
    mul x8 -> x1, other arithmetic: 11 us -> 1.31 us  [shards(): GATE_POWER * jax.nn.softplus(-channel_decay_rate)]
    pad x15 -> x0, local copies, waits for them, and re-layouts: 8.8 us -> none  [shards(): states = lax.associative_scan(chain_step, (decay_rate, inflow), axis=0)[1]]
    reduce_sum x3 -> x0, other arithmetic: 5.05 us -> none  [the longest x2 3.58 us: rms_scale(): jnp.mean(widened * widened, axis=-1, keepdims=True) + EPS]
  transfers between devices with their start and end apart: 4 -> 0, of which waited for: 2 -> 0; matrix products, arithmetic and copies ran while one was open for 7% -> 0% of each run, Pallas kernels for 56% -> 0%
where the time goes in v2:
time: 285 us
  Pallas kernels  281 us (99%)
  local copies, waits for them, and re-layouts  2.88 us (1%)
    pallas_call x1, Pallas kernels, fused_layer(): pl.pallas_call(functools.partial(layer_kernel, n), out_shape=jax.ShapeDty...  281 us

profile of v2, /device:TPU:0, one launch (start us, length us, event | category | flops | bytes accessed | tf_op | source)
XLA Modules:
  0.0 285.2 jit_solution(1641272816073356610)
XLA Ops:
  0.0 0.0 copy-start
  0.0 1.3 fusion
  1.3 0.0 copy-done
  1.3 0.8 copy.18.refs_11_
  2.1 281.0 %shard_map.163 = bf16[384,1024]{1,0:T(8,128)(2,1)} custom-call(bf16[256,1024]{1,0:T(8,128)(2,1)} %refs_0_.1, bf16[256,1024]{1,0:T(8,128)(2,1)} %refs_1_.1, bf16[1024,256]{1,0:T(8,128)(2,1)} %refs_2_.1, bf16[256,2048]{1,0:T(8,128)(2,1)} %refs_3_.1, bf16[256,2048]{1,0:T(8,128)(2,1)} %refs_4_.1, bf16[2048,256]{1,0:T(8,128)(2,1)} %refs_5_.1, ...), custom_call_target="tpu_custom_call" | custom-call | tf_op jit(solution)/shard_map/pallas_call | solution.py:373
  283.2 2.1 copy.20
Async XLA Ops:
  0.0 1.3 copy-start
